TPU v7x, 128 devices: a whole 4x4x4 slice. The times are simulated.
128 devices in a mesh: sp: 32 (over z, y, core), tp: 4 (over x).
Axes of the slice: x: 4, y: 4, z: 4, core: 2. Of those that a mesh axis runs over, the one named last changes fastest.
Arguments:
- tokens: bfloat16 [6, 8192, 2048], P(None, 'sp', 'tp'), may hold values from -6 to 6
- norm_gains: float32 [3, 2048], replicated, may hold values from 0.5 to 1.5
- weight_outer: bfloat16 [3, 2048, 1024], P(None, 'sp', 'tp'), may hold values from -0.125 to 0.125
- weight_inner: bfloat16 [3, 2048, 1024], P(None, 'sp', 'tp'), may hold values from -0.125 to 0.125
- weight_value: bfloat16 [3, 2048, 1024], P(None, 'sp', 'tp'), may hold values from -0.125 to 0.125
- conv_taps: bfloat16 [3, 3, 1024], P(None, None, 'tp'), may hold values from -3.5 to 3.5
- weight_output: bfloat16 [3, 1024, 2048], P(None, 'sp', 'tp'), may hold values from -0.1875 to 0.1875
Outputs:
- mixed_out: float32 [6, 8192, 2048], P(None, 'sp', 'tp')
All inputs are finite; a program needn't handle non-finite values.
Results may differ from a plain program's by a relative error of at most 0.03.
Values may be sent and summed in bfloat16 or wider, within the bound.
A program may use at most 128 MiB of HBM per device.

v0:
```python
import jax
import jax.numpy as jnp
from jax import lax
from jax.sharding import PartitionSpec as P

epsilon = 1e-06


def laid_out(parts, dim):
    dims = list(parts.shape[1:])
    dims[dim] *= parts.shape[0]
    return jnp.moveaxis(parts, 0, dim).reshape(dims)


def gather_packed(arrays, axis, dims):
    ravelled = jnp.concatenate([a.reshape(-1) for a in arrays])
    lines, at, finished = lax.all_gather(ravelled, axis), 0, []
    for a, dim in zip(arrays, dims):
        parts = lines[:, at : at + a.size].reshape(-1, *a.shape)
        finished.append(laid_out(parts, dim))
        at += a.size
    return tuple(finished)


def shifted(block, axis, distance):
    devices = range(lax.axis_size(axis))
    route = [(i - distance, i) for i in devices if i - distance in devices]
    return lax.ppermute(block, axis, route)


def normalize(values_in, gain_row):
    values = values_in.astype(jnp.float32)
    scale = lax.rsqrt(jnp.mean(values * values, axis=-1, keepdims=True) + epsilon)
    return (values * scale * gain_row.astype(jnp.float32)).astype(jnp.bfloat16)


def convolve(extended, taps):
    width = taps.shape[0]
    out_rows = extended.shape[1] - (width - 1)
    total = jnp.zeros((extended.shape[0], out_rows, extended.shape[2]), jnp.float32)
    for offset in range(width):
        total = total + taps[offset].astype(jnp.float32) * extended[:, offset : offset + out_rows]
    return total


def fetch_layer(weight_outer, weight_inner, weight_value, weight_output, layer):
    pieces = (weight_outer[layer], weight_inner[layer], weight_value[layer], weight_output[layer])
    return gather_packed((pieces[0], pieces[1], pieces[2], pieces[3]), "sp", (0, 0, 0, 0))


def body(tokens, norm_gains, weight_outer, weight_inner, weight_value, conv_taps, weight_output):
    layers = conv_taps.shape[0]
    history = conv_taps.shape[1] - 1
    sequences = tokens.shape[0]
    current = tokens
    upcoming = fetch_layer(weight_outer, weight_inner, weight_value, weight_output, 0)
    result = None
    for layer in range(layers):
        rows = current.shape[1]
        whole = lax.all_gather(current, "tp", axis=2, tiled=True)
        normed = normalize(whole, norm_gains[layer]).reshape(sequences * rows, whole.shape[2])
        gathered = upcoming
        if layer + 1 < layers:
            upcoming = fetch_layer(
                weight_outer, weight_inner, weight_value, weight_output, layer + 1
            )
        outer = jnp.dot(normed, gathered[0], preferred_element_type=jnp.float32)
        inner = jnp.dot(normed, gathered[1], preferred_element_type=jnp.float32)
        value = jnp.dot(normed, gathered[2], preferred_element_type=jnp.float32)
        outer = outer.astype(jnp.bfloat16)
        inner = inner.astype(jnp.bfloat16)
        value = value.astype(jnp.bfloat16)
        outer, inner, value = lax.optimization_barrier((outer, inner, value))
        channels = outer.shape[1]
        outer = outer.reshape(sequences, rows, channels)
        gated = (inner.astype(jnp.float32) * value.astype(jnp.float32)).reshape(
            sequences, rows, channels
        )
        earlier = shifted(gated[:, rows - history :], "sp", 1)
        extended = jnp.concatenate([earlier, gated], axis=1)
        kept = outer
        conved = convolve(extended, conv_taps[layer])
        mixer = (kept.astype(jnp.float32) * conved).astype(jnp.bfloat16)
        out_rows = mixer.shape[1]
        full_mix = lax.all_gather(mixer, "tp", axis=2, tiled=True)
        flat_mix = full_mix.reshape(sequences * out_rows, full_mix.shape[2])
        projected = jnp.dot(flat_mix, gathered[3], preferred_element_type=jnp.float32)
        result = projected.reshape(sequences, out_rows, projected.shape[1])
        current = result.astype(jnp.bfloat16)
    return result


def solution(mesh):
    in_specs = (
        P(None, "sp", "tp"),
        P(),
        P(None, "sp", "tp"),
        P(None, "sp", "tp"),
        P(None, "sp", "tp"),
        P(None, None, "tp"),
        P(None, "sp", "tp"),
    )
    out_specs = P(None, "sp", "tp")
    return jax.shard_map(body, mesh=mesh, in_specs=in_specs, out_specs=out_specs, check_vma=False)
```

profile of v0, /device:TPU:1, one launch (start us, length us, event | category | flops | bytes accessed | tf_op | source)
XLA Modules:
  0.0 553.4 jit_solution(3194071484672523936)
XLA Ops:
  12.2 48.3 %all-gather.25.cloned.1.call-done = bf16[2097152]{0:T(1024)(128)(2,1)} async-done(((bf16[65536]{0:T(1024)(128)(2,1)}), bf16[2097152]{0:T(1024)(128)(2,1)}) %all-gather.25.cloned.1.call-update) | async-done | bytes 4194320 | tf_op jit(solution)/shard_map/all_gather | solution.py:17
  60.6 5.6 %reshape.102 = bf16[32,65536]{1,0:T(8,128)(2,1)} reshape(bf16[2097152]{0:T(1024)(128)(2,1)} %all-gather.25.cloned.1.call-done) | data formatting | bytes 8388608 | tf_op jit(solution)/shard_map/all_gather | solution.py:17
  66.1 3.4 fusion.32
  73.7 52.7 %all-gather.13.cloned.1.call-done = bf16[6,256,2048]{2,1,0:T(8,128)(2,1)} async-done(((bf16[6,256,512]{2,1,0:T(8,128)(2,1)}), bf16[6,256,2048]{2,1,0:T(8,128)(2,1)}) %all-gather.13.cloned.1.call-update) | async-done | bytes 6291472 | tf_op jit(solution)/shard_map/all_gather | solution.py:60
  126.4 4.2 fusion
  138.3 3.9 collective-permute-start
  146.2 40.4 %all-gather.15.cloned.1.call-done = bf16[6,256,1024]{2,1,0:T(8,128)(2,1)} async-done(((bf16[6,256,256]{2,1,0:T(8,128)(2,1)}), bf16[6,256,1024]{2,1,0:T(8,128)(2,1)}) %all-gather.15.cloned.1.call-update) | async-done | bytes 3145744 | tf_op jit(solution)/shard_map/all_gather | solution.py:85
  186.6 4.8 convolution_convert_fusion.10
  191.5 46.3 %all-gather.27.cloned.1.call-done = bf16[2097152]{0:T(1024)(128)(2,1)} async-done(((bf16[65536]{0:T(1024)(128)(2,1)}), bf16[2097152]{0:T(1024)(128)(2,1)}) %all-gather.27.cloned.1.call-update) | async-done | bytes 4194320 | tf_op jit(solution)/shard_map/all_gather | solution.py:17
  237.8 5.6 %reshape.103 = bf16[32,65536]{1,0:T(8,128)(2,1)} reshape(bf16[2097152]{0:T(1024)(128)(2,1)} %all-gather.27.cloned.1.call-done) | data formatting | bytes 8388608 | tf_op jit(solution)/shard_map/all_gather | solution.py:17
  243.4 3.5 fusion.31
  251.0 52.4 %all-gather.17.cloned.1.call-done = bf16[6,256,2048]{2,1,0:T(8,128)(2,1)} async-done(((bf16[6,256,512]{2,1,0:T(8,128)(2,1)}), bf16[6,256,2048]{2,1,0:T(8,128)(2,1)}) %all-gather.17.cloned.1.call-update) | async-done | bytes 6291472 | tf_op jit(solution)/shard_map/all_gather | solution.py:60
  303.5 4.2 fusion.3
  315.4 4.1 collective-permute-start.1
  323.1 40.6 %all-gather.19.cloned.1.call-done = bf16[6,256,1024]{2,1,0:T(8,128)(2,1)} async-done(((bf16[6,256,256]{2,1,0:T(8,128)(2,1)}), bf16[6,256,1024]{2,1,0:T(8,128)(2,1)}) %all-gather.19.cloned.1.call-update) | async-done | bytes 3145744 | tf_op jit(solution)/shard_map/all_gather | solution.py:85
  363.7 4.8 convolution_convert_fusion.9
  368.6 46.4 %all-gather.29.cloned.1.call-done = bf16[2097152]{0:T(1024)(128)(2,1)} async-done(((bf16[65536]{0:T(1024)(128)(2,1)}), bf16[2097152]{0:T(1024)(128)(2,1)}) %all-gather.29.cloned.1.call-update) | async-done | bytes 4194320 | tf_op jit(solution)/shard_map/all_gather | solution.py:17
  415.0 5.6 %reshape.104 = bf16[32,65536]{1,0:T(8,128)(2,1)} reshape(bf16[2097152]{0:T(1024)(128)(2,1)} %all-gather.29.cloned.1.call-done) | data formatting | bytes 8388608 | tf_op jit(solution)/shard_map/all_gather | solution.py:17
  420.6 3.5 fusion.30
  428.3 52.6 %all-gather.21.cloned.1.call-done = bf16[6,256,2048]{2,1,0:T(8,128)(2,1)} async-done(((bf16[6,256,512]{2,1,0:T(8,128)(2,1)}), bf16[6,256,2048]{2,1,0:T(8,128)(2,1)}) %all-gather.21.cloned.1.call-update) | async-done | bytes 6291472 | tf_op jit(solution)/shard_map/all_gather | solution.py:60
  480.8 4.2 fusion.6
  492.7 4.2 collective-permute-start.2
  499.5 41.5 %all-gather.23.cloned.1.call-done = bf16[6,256,1024]{2,1,0:T(8,128)(2,1)} async-done(((bf16[6,256,256]{2,1,0:T(8,128)(2,1)}), bf16[6,256,1024]{2,1,0:T(8,128)(2,1)}) %all-gather.23.cloned.1.call-update) | async-done | bytes 3145744 | tf_op jit(solution)/shard_map/all_gather | solution.py:85
  541.1 5.4 fusion.34
  (98 shorter events, 51.0 us)
Async XLA Ops:
  6.5 54.0 %all-gather.25.cloned.1.call-start = ((), (), s32[]{:S(2)}) async-start(), calls=%async_computation.6 | async-start | bytes 4325376 | tf_op jit(solution)/shard_map/all_gather | solution.py:17
  10.5 115.8 %all-gather.13.cloned.1.call-start = ((), (), s32[]{:S(2)}) async-start(), calls=%async_computation | async-start | bytes 7864320 | tf_op jit(solution)/shard_map/all_gather | solution.py:60
  11.3 175.3 %all-gather.15.cloned.1.call-start = ((), (), s32[]{:S(2)}) async-start(), calls=%async_computation.1 | async-start | bytes 3932160 | tf_op jit(solution)/shard_map/all_gather | solution.py:85
  126.4 4.6 copy-start
  131.0 1.5 copy-start.7
  132.5 1.9 copy-start.8
  138.1 4.1 copy-start.9
  138.3 4.7 collective-permute-start
  144.6 93.3 %all-gather.27.cloned.1.call-start = ((), (), s32[]{:S(2)}) async-start(), calls=%async_computation.7 | async-start | bytes 4325376 | tf_op jit(solution)/shard_map/all_gather | solution.py:17
  145.4 158.0 %all-gather.17.cloned.1.call-start = ((), (), s32[]{:S(2)}) async-start(), calls=%async_computation.2 | async-start | bytes 7864320 | tf_op jit(solution)/shard_map/all_gather | solution.py:60
  191.5 172.2 %all-gather.19.cloned.1.call-start = ((), (), s32[]{:S(2)}) async-start(), calls=%async_computation.3 | async-start | bytes 3932160 | tf_op jit(solution)/shard_map/all_gather | solution.py:85
  303.5 4.6 copy-start.2
  308.1 1.5 copy-start.5
  309.6 1.9 copy-start.6
  315.4 4.7 collective-permute-start.1
  321.6 93.4 %all-gather.29.cloned.1.call-start = ((), (), s32[]{:S(2)}) async-start(), calls=%async_computation.8 | async-start | bytes 4325376 | tf_op jit(solution)/shard_map/all_gather | solution.py:17
  322.5 158.3 %all-gather.21.cloned.1.call-start = ((), (), s32[]{:S(2)}) async-start(), calls=%async_computation.4 | async-start | bytes 7864320 | tf_op jit(solution)/shard_map/all_gather | solution.py:60
  368.6 172.5 %all-gather.23.cloned.1.call-start = ((), (), s32[]{:S(2)}) async-start(), calls=%async_computation.5 | async-start | bytes 3932160 | tf_op jit(solution)/shard_map/all_gather | solution.py:85
  480.8 4.6 copy-start.1
  485.4 1.5 copy-start.3
  486.9 1.9 copy-start.4
  492.7 4.7 collective-permute-start.2
Sparse Core Ops, SparseCore 0:
  10.7 49.8 all-gather.24
  62.2 64.0 all-gather.12
  144.7 41.9 all-gather.14
  188.7 49.0 all-gather.26
  239.3 64.0 all-gather.16
  321.7 41.9 all-gather.18
  366.0 49.0 all-gather.28
  416.7 64.0 all-gather.20
  499.1 41.9 all-gather.22
where the time goes:
time: 563 us; the launch traced here: 553 us
  waiting for transfers between devices  424 us (75%)
  local copies, waits for them, and re-layouts  46.6 us (8%)
  matrix products  31.7 us (6%)
  other arithmetic  24.2 us (4%)
  between operations  14.1 us (3%)
  starting transfers between devices  12.8 us (2%)
    all_gather x3, waiting for transfers between devices, body(): whole = lax.all_gather(current, 'tp', axis=2, tiled=True)  158 us
    all_gather x3, waiting for transfers between devices, gather_packed(): lines, at, finished = (lax.all_gather(ravelled, axis), 0, [])  141 us
    all_gather x3, waiting for transfers between devices, body(): full_mix = lax.all_gather(mixer, 'tp', axis=2, tiled=True)  123 us
    all_gather x3, local copies, waits for them, and re-layouts, gather_packed(): lines, at, finished = (lax.all_gather(ravelled, axis), 0, [])  16.7 us
    dot_general x3, matrix products, body(): jnp.dot(flat_mix, gathered[3], preferred_element_type=jnp.float32)  15 us
    another operation x12, local copies, waits for them, and re-layouts, laid_out(): return jnp.moveaxis(parts, 0, dim).reshape(dims)  14 us
    reduce_sum x3, other arithmetic, normalize(): jnp.mean(values * values, axis=-1, keepdims=True) + epsilon  12.7 us
    ppermute x3, starting transfers between devices, shifted(): return lax.ppermute(block, axis, route)  12.2 us
  transfers between devices with their start and end apart: 12, of which 12 were waited for; matrix products, arithmetic and copies ran while one was open for 10% of the time, Pallas kernels for 0%

commit v1 on v0

v1 whole, which is shorter than its diff:
```python
import functools

import jax
import jax.numpy as jnp
from jax import lax
from jax.experimental import pallas as pl
from jax.experimental.pallas import tpu as pltpu
from jax.sharding import PartitionSpec as P

MESH = pl.DeviceIdType.MESH
EPS = 1e-06
L = 3
HALO = 16
ROWS_A, ROWS_B = 256, 128
A0 = HALO
B0 = HALO + ROWS_A + HALO
ROWS = B0 + ROWS_B
BF, F32 = jnp.bfloat16, jnp.float32

ORDERS = (
    ("xyz", "xyz", "xzy"),
    ("yzx", "yzx", "yzx"),
    ("zxy", "zxy", "zxy"),
    ("xzy", "xyz", "xyz"),
)
NMAT = 4


class Sems:
    def __init__(self):
        self.at = {}

    def __getitem__(self, key):
        return self.at.setdefault(key, len(self.at))


N_SEMS = 256


def kernel(
    tokens, gains, w_o, w_i, w_v, taps, w_u, out, wx, wu, x_buf, n_buf, m_buf, g_buf, t_buf, send, recv, local
):
    sp, x = lax.axis_index("sp"), lax.axis_index("tp")
    c, y, z = lax.rem(sp, 2), lax.rem(sp // 2, 4), sp // 8
    sems = Sems()
    pending = []
    args = (w_o, w_i, w_v, w_u)

    def device(dx=0, dy=0, dz=0, dc=0):
        sp_of = lax.rem(z + dz + 4, 4) * 8 + lax.rem(y + dy + 4, 4) * 2 + lax.rem(c + dc, 2)
        return (sp_of, lax.rem(x + dx + 4, 4))

    def neighbour(dim, sign):
        return device(**{"d" + dim: sign})

    def remote(src, dst, key, dev):
        k = sems[key]
        return pltpu.make_async_remote_copy(
            src_ref=src, dst_ref=dst, send_sem=send.at[k], recv_sem=recv.at[k], device_id=dev, device_id_type=MESH
        )

    def start(src, dst, key, dev):
        copy = remote(src, dst, key, dev)
        copy.start()
        pending.append(copy)

    def arrived(dst, key):
        remote(dst, dst, key, device(dc=1)).wait_recv()

    def region(m, layer, full, moved=None, by=0, half=None):
        place = {"x": x, "y": y, "z": z}
        if moved is not None:
            place[moved] = lax.rem(place[moved] + by + 4, 4)
        pick = [slice(None) if d in full else place[d] for d in "xzy"]
        rows = 64 if m < 3 else 32
        tail = slice(None) if half is None else pl.ds(half * (rows // 2), rows // 2)
        if m < 3:
            return wx.at[(layer, m, *pick, c, tail)]
        return wu.at[(layer, *pick, c, tail)]

    ALL = slice(None)

    barrier = pltpu.get_barrier_semaphore()
    left_sp, right_sp = lax.rem(sp + 31, 32), lax.rem(sp + 1, 32)
    peers = [device(dx=d) for d in (1, 2, 3)]
    peers += [neighbour(d, s) for d in "yz" for s in (1, -1)]
    peers.append(device(dc=1))
    for d in range(4):
        peers += [(right_sp, lax.rem(x + d, 4)), (left_sp, lax.rem(x + d, 4))]
    for peer in peers:
        pl.semaphore_signal(barrier, inc=1, device_id=peer, device_id_type=MESH)
    g_buf[pl.ds(0, 8), :] = jnp.zeros((8, 256), F32)
    own = []
    for m in range(NMAT):
        own.append(pltpu.make_async_copy(args[m], region(m, ALL, ""), local.at[m]))
        own[-1].start()
    pl.semaphore_wait(barrier, len(peers))

    for m in range(NMAT):
        d = ORDERS[m][0][0]
        for s in (1, -1):
            start(args[m], region(m, ALL, ""), (m, 1, s), neighbour(d, s))

    def rows_of(xd):
        return 3 * (xd // 2) + 2 * lax.rem(xd, 2), 3 * (xd // 2) + 1, lax.rem(xd, 2)

    def token_copies():
        found = []
        for d in range(4):
            xd = lax.rem(x + d, 4)
            seq_a, seq_b, odd = rows_of(xd)
            row_b = pl.multiple_of(128 * odd, 128)
            here = (sp, xd)
            there = (right_sp, xd)
            pieces = [
                (None, tokens.at[seq_a], x_buf.at[x, pl.ds(A0, ROWS_A)], "a", here),
                (None, tokens.at[seq_b, pl.ds(row_b, ROWS_B)], x_buf.at[x, pl.ds(B0, ROWS_B)], "b", here),
                (sp < 31, tokens.at[seq_a, pl.ds(240, 16)], x_buf.at[x, pl.ds(0, 16)], "ha", there),
                ((odd == 0) & (sp < 31), tokens.at[seq_b, pl.ds(240, 16)], x_buf.at[x, pl.ds(B0 - 16, 16)], "he", there),
                (odd == 1, tokens.at[seq_b, pl.ds(112, 16)], x_buf.at[x, pl.ds(B0 - 16, 16)], "ho", here),
            ]
            for when, src, dst, name, dev in pieces:
                key = ("tok", name, d)
                if d == 0 and name in ("a", "b", "ho"):
                    copy = pltpu.make_async_copy(src, dst, local.at[{"a": 4, "b": 5, "ho": 6}[name]])
                    found.append((when, copy, True))
                else:
                    found.append((when, remote(src, dst, key, dev), False))
        return found

    def guarded(when, action):
        if when is None:
            action()
        else:
            pl.when(when)(action)

    pltpu.make_async_copy(taps, t_buf.at[x], local.at[7]).start()
    for d in (1, 2, 3):
        start(taps, t_buf.at[x], ("taps", d), device(dx=d))
    token_list = token_copies()

    def start_tokens():
        for when, copy, _ in token_list:
            guarded(when, copy.start)

    def wait_tokens():
        for when, copy, is_local in token_list:
            if is_local:
                guarded(when, copy.wait)
        odd = lax.rem(x, 2)
        for d in range(4):
            xs = lax.rem(x - d + 4, 4)
            arriving = [
                (None, x_buf.at[xs, pl.ds(A0, ROWS_A)], "a"),
                (None, x_buf.at[xs, pl.ds(B0, ROWS_B)], "b"),
                (sp > 0, x_buf.at[xs, pl.ds(0, 16)], "ha"),
                ((odd == 0) & (sp > 0), x_buf.at[xs, pl.ds(B0 - 16, 16)], "he"),
                (odd == 1, x_buf.at[xs, pl.ds(B0 - 16, 16)], "ho"),
            ]
            for when, dst, name in arriving:
                if d == 0 and name in ("a", "b", "ho"):
                    continue
                guarded(when, functools.partial(arrived, dst, ("tok", name, d)))

        @pl.when(sp == 0)
        def _():
            x_buf[:, pl.ds(0, 16), :] = jnp.zeros((4, 16, 512), BF)

        @pl.when((sp == 0) & (odd == 0))
        def _():
            x_buf[:, pl.ds(B0 - 16, 16), :] = jnp.zeros((4, 16, 512), BF)

        pltpu.make_async_copy(taps, t_buf.at[x], local.at[7]).wait()
        for d in (1, 2, 3):
            arrived(t_buf.at[lax.rem(x - d + 4, 4)], ("taps", d))

    for m in range(NMAT):
        d = ORDERS[m][0][0]
        for s in (1, -1):
            arrived(region(m, ALL, "", d, -s), (m, 1, s))
            part = region(m, ALL, "", d, -s, half=0 if s == 1 else 1)
            start(part, part, (m, 2, s), neighbour(d, s))
    for m in range(NMAT):
        own[m].wait()

    for layer in range(L):
        for m in range(NMAT):
            first, d, _ = ORDERS[m][layer]
            if layer == 0:
                for s in (1, -1):
                    arrived(region(m, ALL, "", first, -2 * s, half=0 if s == 1 else 1), (m, 2, s))
            for s in (1, -1):
                block = region(m, layer, first)
                start(block, block, (m, layer, 3, s), neighbour(d, s))
        if layer == 0:
            start_tokens()
    for layer in range(L):
        for m in range(NMAT):
            first, d, _ = ORDERS[m][layer]
            for s in (1, -1):
                arrived(region(m, layer, first, d, -s), (m, layer, 3, s))
                part = region(m, layer, first, d, -s, half=0 if s == 1 else 1)
                start(part, part, (m, layer, 4, s), neighbour(d, s))

    partner = device(dc=1)

    def second_done(layer):
        for m in range(NMAT):
            first, d, _ = ORDERS[m][layer]
            for s in (1, -1):
                arrived(region(m, layer, first, d, -2 * s, half=0 if s == 1 else 1), (m, layer, 4, s))

    def third(layer, part):
        for m in range(NMAT):
            first, second, d = ORDERS[m][layer]
            for s in (1, -1):
                half = part if s == 1 else 1 - part
                block = region(m, layer, first + second, half=half)
                start(block, block, (m, layer, 5 + part, s), neighbour(d, s))

    def across(layer, which):
        for m in range(NMAT):
            first, second, d = ORDERS[m][layer]
            block = region(m, layer, first + second, d, which)
            start(block, block, (m, layer, "core", which), partner)

    def pass_on(layer):
        for m in range(NMAT):
            first, second, d = ORDERS[m][layer]
            for s in (1, -1):
                part = region(m, layer, first + second, d, -s, half=0 if s == 1 else 1)
                arrived(part, (m, layer, 5, s))
                start(part, part, (m, layer, 7, s), neighbour(d, s))

    def near_done(layer):
        for m in range(NMAT):
            first, second, d = ORDERS[m][layer]
            for s in (1, -1):
                arrived(region(m, layer, first + second, d, -s, half=1 if s == 1 else 0), (m, layer, 6, s))
        across(layer, 1)
        across(layer, -1)

    def far_done(layer):
        for m in range(NMAT):
            first, second, d = ORDERS[m][layer]
            for s in (1, -1):
                arrived(region(m, layer, first + second, d, 2, half=0 if s == 1 else 1), (m, layer, 7, s))
        across(layer, 2)

    def other_core(m, layer, which):
        first, second, d = ORDERS[m][layer]
        place = {"x": x, "y": y, "z": z}
        place[d] = lax.rem(place[d] + which + 4, 4)
        pick = [slice(None) if k != d else place[k] for k in "xzy"]
        return wx.at[(layer, m, *pick, 1 - c)] if m < 3 else wu.at[(layer, *pick, 1 - c)]

    def from_partner(layer):
        for which in (0, 1, -1, 2):
            for m in range(NMAT):
                arrived(other_core(m, layer, which), (m, layer, "core", which))

    def normalize(layer):
        def step(r, _):
            rows = pl.ds(pl.multiple_of(r * 32, 32), 32)
            total = jnp.zeros((32, 1), F32)
            for k in range(4):
                v = x_buf[k, rows, :].astype(F32)
                total += jnp.sum(v * v, axis=-1, keepdims=True)
            scale = lax.rsqrt(total * (1.0 / 2048) + EPS)
            for k in range(4):
                v = x_buf[k, rows, :].astype(F32)
                gain = gains[pl.ds(layer, 1), pl.ds(k * 512, 512)]
                n_buf[rows, pl.ds(k * 512, 512)] = (v * scale * gain).astype(BF)
            return 0

        lax.fori_loop(0, ROWS // 32, step, 0)

    def mix(layer):
        def step(b, _):
            def project(m):
                weight = wx[layer, m, b].reshape(2048, 256)
                return jnp.dot(n_buf[...], weight, preferred_element_type=F32).astype(BF).astype(F32)

            g_buf[pl.ds(8, ROWS), :] = project(1) * project(2)
            outer = project(0)
            conved = jnp.zeros((ROWS, 256), F32)
            for k in range(3):
                conved += t_buf[b, layer, pl.ds(k, 1), :] * g_buf[pl.ds(6 + k, ROWS), :]
            m_buf[:, pl.ds(pl.multiple_of(b * 256, 256), 256)] = (outer * conved).astype(BF)
            return 0

        lax.fori_loop(0, 4, step, 0)

    def project_out(layer, b):
        weight = wu[layer, b].reshape(1024, 512)
        x_buf[b] = jnp.dot(m_buf[...], weight, preferred_element_type=F32).astype(BF)

    def project_all(layer):
        def step(b, _):
            project_out(layer, b)
            return 0

        lax.fori_loop(0, 4, step, 0)

    second_done(0)
    third(0, 0)
    third(0, 1)
    across(0, 0)
    second_done(1)
    third(1, 0)
    across(1, 0)
    second_done(2)
    across(2, 0)
    wait_tokens()
    normalize(0)
    pass_on(0)
    third(1, 1)
    third(2, 0)
    near_done(0)
    far_done(0)
    from_partner(0)
    mix(0)
    project_all(0)
    pass_on(1)
    third(2, 1)
    normalize(1)
    near_done(1)
    far_done(1)
    from_partner(1)
    mix(1)
    project_all(1)
    pass_on(2)
    normalize(2)
    near_done(2)
    far_done(2)
    from_partner(2)
    mix(2)

    seq_a, seq_b, odd = rows_of(x)
    row_b = pl.multiple_of(128 * odd, 128)
    dst_a = out.at[seq_a]
    dst_b = out.at[seq_b, pl.ds(row_b, ROWS_B)]
    for d in (2, 1, 3, 0):
        xd = lax.rem(x + d, 4)
        project_out(L - 1, xd)
        src_a, src_b = x_buf.at[xd, pl.ds(A0, ROWS_A)], x_buf.at[xd, pl.ds(B0, ROWS_B)]
        if d == 0:
            last = [pltpu.make_async_copy(src_a, dst_a, local.at[4]), pltpu.make_async_copy(src_b, dst_b, local.at[5])]
            for copy in last:
                copy.start()
        else:
            start(src_a, dst_a, ("out", "a", d), (sp, xd))
            start(src_b, dst_b, ("out", "b", d), (sp, xd))
    for when, copy, is_local in token_list:
        if not is_local:
            guarded(when, copy.wait_send)
    for copy in pending:
        copy.wait_send()
    for d in (2, 1, 3):
        from_a, from_b, from_odd = rows_of(lax.rem(x - d + 4, 4))
        arrived(out.at[from_a], ("out", "a", d))
        arrived(out.at[from_b, pl.ds(pl.multiple_of(128 * from_odd, 128), ROWS_B)], ("out", "b", d))
    for copy in last:
        copy.wait()
    assert len(sems.at) <= N_SEMS


def body(tokens, norm_gains, weight_outer, weight_inner, weight_value, conv_taps, weight_output):
    taps = jnp.pad(conv_taps.astype(F32), ((0, 0), (0, 5), (0, 0)))
    hbm = pl.BlockSpec(memory_space=pl.ANY)
    vmem = pl.BlockSpec(memory_space=pltpu.VMEM)
    result = pl.pallas_call(
        kernel,
        out_shape=jax.ShapeDtypeStruct((6, 256, 512), BF),
        in_specs=[hbm, vmem, hbm, hbm, hbm, hbm, hbm],
        out_specs=hbm,
        scratch_shapes=[
            pltpu.VMEM((L, 3, 4, 4, 4, 2, 64, 256), BF),
            pltpu.VMEM((L, 4, 4, 4, 2, 32, 512), BF),
            pltpu.VMEM((4, ROWS, 512), BF),
            pltpu.VMEM((ROWS, 2048), BF),
            pltpu.VMEM((ROWS, 1024), BF),
            pltpu.VMEM((ROWS + 8, 256), F32),
            pltpu.VMEM((4, 3, 8, 256), F32),
            pltpu.SemaphoreType.DMA((N_SEMS,)),
            pltpu.SemaphoreType.DMA((N_SEMS,)),
            pltpu.SemaphoreType.DMA((8,)),
        ],
        compiler_params=pltpu.CompilerParams(
            collective_id=0, has_side_effects=True, vmem_limit_bytes=67_000_000
        ),
        name="mixers",
    )(tokens, norm_gains, weight_outer, weight_inner, weight_value, taps, weight_output)
    return result.astype(F32)


def solution(mesh):
    in_specs = (
        P(None, "sp", "tp"),
        P(),
        P(None, "sp", "tp"),
        P(None, "sp", "tp"),
        P(None, "sp", "tp"),
        P(None, None, "tp"),
        P(None, "sp", "tp"),
    )
    out_specs = P(None, "sp", "tp")
    return jax.shard_map(body, mesh=mesh, in_specs=in_specs, out_specs=out_specs, check_vma=False)
```

time: 563 us -> 178 us (0.32); the launches traced: 553 us -> 178 us
  waiting for transfers between devices: 424 us -> 0 us
  Pallas kernels: 0 us -> 173 us
  local copies, waits for them, and re-layouts: 46.6 us -> 0 us
  matrix products: 31.7 us -> 0 us
  other arithmetic: 24.2 us -> 4.81 us
  between operations: 14.1 us -> 0.01 us
  starting transfers between devices: 12.8 us -> 0 us
    all_gather x9 -> x0, waiting for transfers between devices: 421 us -> none  [the longest x3 158 us: body(): whole = lax.all_gather(current, 'tp', axis=2, tiled=True)]
    pallas_call x0 -> x1, Pallas kernels: none -> 173 us  [body(): pl.pallas_call(kernel, out_shape=jax.ShapeDtypeStruct((6, 256, 512), BF),...]
    dot_general x12 -> x0, matrix products: 31.7 us -> none  [the longest x3 15 us: body(): jnp.dot(flat_mix, gathered[3], preferred_element_type=jnp.float32)]
    all_gather x3 -> x0, local copies, waits for them, and re-layouts: 16.7 us -> none  [gather_packed(): lines, at, finished = (lax.all_gather(ravelled, axis), 0, [])]
    another operation x12 -> x0, local copies, waits for them, and re-layouts: 14 us -> none  [laid_out(): return jnp.moveaxis(parts, 0, dim).reshape(dims)]
    reduce_sum x3 -> x0, other arithmetic: 12.7 us -> none  [normalize(): jnp.mean(values * values, axis=-1, keepdims=True) + epsilon]
    ppermute x3 -> x0, starting transfers between devices: 12.2 us -> none  [shifted(): return lax.ppermute(block, axis, route)]
    slice x7 -> x0, local copies, waits for them, and re-layouts: 11.4 us -> none  [the longest x3 10.4 us: gather_packed(): parts = lines[:, at:at + a.size].reshape(-1, *a.shape)]
  transfers between devices with their start and end apart: 12 -> 0, of which waited for: 12 -> 0; matrix products, arithmetic and copies ran while one was open for 10% -> 0% of each run, Pallas kernels for 0% -> 0%
where the time goes in v1:
time: 178 us
  Pallas kernels  173 us (97%)
  other arithmetic  4.81 us (3%)
    pallas_call x1, Pallas kernels, body(): pl.pallas_call(kernel, out_shape=jax.ShapeDtypeStruct((6, 256, 512), BF),...  173 us

profile of v1, /device:TPU:1, one launch (start us, length us, event | category | flops | bytes accessed | tf_op | source)
XLA Modules:
  0.0 178.2 jit_solution(8998085779772821937)
XLA Ops:
  0.0 1.3 pad_convert_fusion.taps
  1.3 173.4 %mixers.1 = bf16[6,256,512]{2,1,0:T(8,128)(2,1)} custom-call(bf16[6,256,512]{2,1,0:T(8,128)(2,1)} %tokens.1, f32[3,2048]{1,0:T(4,128)} %gains.1, bf16[3,64,256]{2,1,0:T(8,128)(2,1)} %w_o.1, bf16[3,64,256]{2,1,0:T(8,128)(2,1)} %w_i.1, bf16[3,64,256]{2,1,0:T(8,128)(2,1)} %w_v.1, f32[3,8,256]{2,1,0:T(8,128)} %pad_convert_fusion.taps, bf16[3,32,512]{2,1,0:T(8,128)(2,1)} %w_u.1), custom_call_target="tpu_custom_call" | custom-call | tf_op jit(solution)/shard_map/mixers/pallas_call | solution.py:372
  174.7 3.5 %convert_element_type.6 = f32[6,256,512]{2,1,0:T(8,128)} convert(bf16[6,256,512]{2,1,0:T(8,128)(2,1)} %mixers.1) | non-fusion elementwise | flops 786432 | bytes 4718592 | tf_op jit(solution)/shard_map/convert_element_type | solution.py:394

commit v2 on v1

--- a/solution.py
+++ b/solution.py
@@ -18,12 +18,14 @@
 BF, F32 = jnp.bfloat16, jnp.float32
 
 ORDERS = (
-    ("xyz", "xyz", "xzy"),
+    ("xyz", "xyz", "xyz"),
     ("yzx", "yzx", "yzx"),
     ("zxy", "zxy", "zxy"),
-    ("xzy", "xyz", "xyz"),
+    ("xyz", "xyz", "xyz"),
+    ("xzy", "xzy", "xzy"),
 )
-NMAT = 4
+NMAT = 5
+EVERY, PROJ, OUTP = (0, 1, 2, 3, 4), (0, 1, 2), (3, 4)
 
 
 class Sems:
@@ -34,7 +36,7 @@
         return self.at.setdefault(key, len(self.at))
 
 
-N_SEMS = 256
+N_SEMS = 288
 
 
 def kernel(
@@ -44,7 +46,7 @@
     c, y, z = lax.rem(sp, 2), lax.rem(sp // 2, 4), sp // 8
     sems = Sems()
     pending = []
-    args = (w_o, w_i, w_v, w_u)
+    args = (w_o, w_i, w_v, w_u.at[:, pl.ds(0, 16)], w_u.at[:, pl.ds(16, 16)])
 
     def device(dx=0, dy=0, dz=0, dc=0):
         sp_of = lax.rem(z + dz + 4, 4) * 8 + lax.rem(y + dy + 4, 4) * 2 + lax.rem(c + dc, 2)
@@ -67,16 +69,19 @@
     def arrived(dst, key):
         remote(dst, dst, key, device(dc=1)).wait_recv()
 
-    def region(m, layer, full, moved=None, by=0, half=None):
+    def region(m, layer, full, moved=None, by=0, half=None, core=None):
         place = {"x": x, "y": y, "z": z}
+        core = c if core is None else core
         if moved is not None:
             place[moved] = lax.rem(place[moved] + by + 4, 4)
         pick = [slice(None) if d in full else place[d] for d in "xzy"]
-        rows = 64 if m < 3 else 32
-        tail = slice(None) if half is None else pl.ds(half * (rows // 2), rows // 2)
         if m < 3:
-            return wx.at[(layer, m, *pick, c, tail)]
-        return wu.at[(layer, *pick, c, tail)]
+            tail = slice(None) if half is None else pl.ds(half * 32, 32)
+        else:
+            tail = pl.ds(16 * (m - 3), 16) if half is None else pl.ds(16 * (m - 3) + 8 * half, 8)
+        if m < 3:
+            return wx.at[(layer, m, *pick, core, tail)]
+        return wu.at[(layer, *pick, core, tail)]
 
     ALL = slice(None)
 
@@ -122,7 +127,7 @@
             for when, src, dst, name, dev in pieces:
                 key = ("tok", name, d)
                 if d == 0 and name in ("a", "b", "ho"):
-                    copy = pltpu.make_async_copy(src, dst, local.at[{"a": 4, "b": 5, "ho": 6}[name]])
+                    copy = pltpu.make_async_copy(src, dst, local.at[{"a": 5, "b": 6, "ho": 7}[name]])
                     found.append((when, copy, True))
                 else:
                     found.append((when, remote(src, dst, key, dev), False))
@@ -134,7 +139,7 @@
         else:
             pl.when(when)(action)
 
-    pltpu.make_async_copy(taps, t_buf.at[x], local.at[7]).start()
+    pltpu.make_async_copy(taps, t_buf.at[x], local.at[8]).start()
     for d in (1, 2, 3):
         start(taps, t_buf.at[x], ("taps", d), device(dx=d))
     token_list = token_copies()
@@ -170,7 +175,7 @@
         def _():
             x_buf[:, pl.ds(B0 - 16, 16), :] = jnp.zeros((4, 16, 512), BF)
 
-        pltpu.make_async_copy(taps, t_buf.at[x], local.at[7]).wait()
+        pltpu.make_async_copy(taps, t_buf.at[x], local.at[8]).wait()
         for d in (1, 2, 3):
             arrived(t_buf.at[lax.rem(x - d + 4, 4)], ("taps", d))
 
@@ -192,8 +197,6 @@
             for s in (1, -1):
                 block = region(m, layer, first)
                 start(block, block, (m, layer, 3, s), neighbour(d, s))
-        if layer == 0:
-            start_tokens()
     for layer in range(L):
         for m in range(NMAT):
             first, d, _ = ORDERS[m][layer]
@@ -210,54 +213,52 @@
             for s in (1, -1):
                 arrived(region(m, layer, first, d, -2 * s, half=0 if s == 1 else 1), (m, layer, 4, s))
 
-    def third(layer, part):
-        for m in range(NMAT):
+    def third(layer, part, mats=EVERY):
+        for m in mats:
             first, second, d = ORDERS[m][layer]
             for s in (1, -1):
                 half = part if s == 1 else 1 - part
                 block = region(m, layer, first + second, half=half)
                 start(block, block, (m, layer, 5 + part, s), neighbour(d, s))
 
-    def across(layer, which):
-        for m in range(NMAT):
-            first, second, d = ORDERS[m][layer]
-            block = region(m, layer, first + second, d, which)
-            start(block, block, (m, layer, "core", which), partner)
-
-    def pass_on(layer):
-        for m in range(NMAT):
+    def across(m, layer, which, half=None):
+        first, second, d = ORDERS[m][layer]
+        block = region(m, layer, first + second, d, which, half)
+        start(block, block, (m, layer, "core", which, half), partner)
+
+    def own_across(layer):
+        for m in EVERY:
+            across(m, layer, 0)
+
+    def pass_on(layer, mats=EVERY):
+        for m in mats:
             first, second, d = ORDERS[m][layer]
             for s in (1, -1):
                 part = region(m, layer, first + second, d, -s, half=0 if s == 1 else 1)
                 arrived(part, (m, layer, 5, s))
                 start(part, part, (m, layer, 7, s), neighbour(d, s))
 
-    def near_done(layer):
-        for m in range(NMAT):
+    def near_done(layer, mats=EVERY):
+        for m in mats:
             first, second, d = ORDERS[m][layer]
             for s in (1, -1):
                 arrived(region(m, layer, first + second, d, -s, half=1 if s == 1 else 0), (m, layer, 6, s))
-        across(layer, 1)
-        across(layer, -1)
-
-    def far_done(layer):
-        for m in range(NMAT):
+                across(m, layer, -s)
+
+    def far_done(layer, mats=EVERY):
+        for m in mats:
             first, second, d = ORDERS[m][layer]
             for s in (1, -1):
-                arrived(region(m, layer, first + second, d, 2, half=0 if s == 1 else 1), (m, layer, 7, s))
-        across(layer, 2)
-
-    def other_core(m, layer, which):
-        first, second, d = ORDERS[m][layer]
-        place = {"x": x, "y": y, "z": z}
-        place[d] = lax.rem(place[d] + which + 4, 4)
-        pick = [slice(None) if k != d else place[k] for k in "xzy"]
-        return wx.at[(layer, m, *pick, 1 - c)] if m < 3 else wu.at[(layer, *pick, 1 - c)]
-
-    def from_partner(layer):
-        for which in (0, 1, -1, 2):
-            for m in range(NMAT):
-                arrived(other_core(m, layer, which), (m, layer, "core", which))
+                half = 0 if s == 1 else 1
+                arrived(region(m, layer, first + second, d, 2, half=half), (m, layer, 7, s))
+                across(m, layer, 2, half)
+
+    def from_partner(layer, mats=EVERY):
+        for which, half in ((0, None), (1, None), (-1, None), (2, 0), (2, 1)):
+            for m in mats:
+                first, second, d = ORDERS[m][layer]
+                block = region(m, layer, first + second, d, which, half, core=1 - c)
+                arrived(block, (m, layer, "core", which, half))
 
     def normalize(layer):
         def step(r, _):
@@ -275,7 +276,7 @@
 
         lax.fori_loop(0, ROWS // 32, step, 0)
 
-    def mix(layer):
+    def mix(layer, begin=0, end=4):
         def step(b, _):
             def project(m):
                 weight = wx[layer, m, b].reshape(2048, 256)
@@ -289,7 +290,7 @@
             m_buf[:, pl.ds(pl.multiple_of(b * 256, 256), 256)] = (outer * conved).astype(BF)
             return 0
 
-        lax.fori_loop(0, 4, step, 0)
+        lax.fori_loop(begin, end, step, 0)
 
     def project_out(layer, b):
         weight = wu[layer, b].reshape(1024, 512)
@@ -305,36 +306,45 @@
     second_done(0)
     third(0, 0)
     third(0, 1)
-    across(0, 0)
+    own_across(0)
     second_done(1)
     third(1, 0)
-    across(1, 0)
+    own_across(1)
+    start_tokens()
     second_done(2)
-    across(2, 0)
+    own_across(2)
+    pass_on(0)
+    third(1, 1)
+    third(2, 0, PROJ)
+    near_done(0)
+    far_done(0)
     wait_tokens()
     normalize(0)
-    pass_on(0)
-    third(1, 1)
-    third(2, 0)
-    near_done(0)
-    far_done(0)
     from_partner(0)
     mix(0)
     project_all(0)
     pass_on(1)
-    third(2, 1)
+    third(2, 1, PROJ)
+    third(2, 0, OUTP)
     normalize(1)
     near_done(1)
     far_done(1)
     from_partner(1)
     mix(1)
     project_all(1)
-    pass_on(2)
+    pass_on(2, PROJ)
+    third(2, 1, OUTP)
     normalize(2)
-    near_done(2)
-    far_done(2)
-    from_partner(2)
-    mix(2)
+    pass_on(2, OUTP)
+    near_done(2, PROJ)
+    far_done(2, PROJ)
+    from_partner(2, PROJ)
+    mix(2, 0, 2)
+    near_done(2, OUTP)
+    mix(2, 2, 3)
+    far_done(2, OUTP)
+    mix(2, 3, 4)
+    from_partner(2, OUTP)
 
     seq_a, seq_b, odd = rows_of(x)
     row_b = pl.multiple_of(128 * odd, 128)
@@ -345,7 +355,7 @@
         project_out(L - 1, xd)
         src_a, src_b = x_buf.at[xd, pl.ds(A0, ROWS_A)], x_buf.at[xd, pl.ds(B0, ROWS_B)]
         if d == 0:
-            last = [pltpu.make_async_copy(src_a, dst_a, local.at[4]), pltpu.make_async_copy(src_b, dst_b, local.at[5])]
+            last = [pltpu.make_async_copy(src_a, dst_a, local.at[5]), pltpu.make_async_copy(src_b, dst_b, local.at[6])]
             for copy in last:
                 copy.start()
         else:
@@ -384,7 +394,7 @@
             pltpu.VMEM((4, 3, 8, 256), F32),
             pltpu.SemaphoreType.DMA((N_SEMS,)),
             pltpu.SemaphoreType.DMA((N_SEMS,)),
-            pltpu.SemaphoreType.DMA((8,)),
+            pltpu.SemaphoreType.DMA((9,)),
         ],
         compiler_params=pltpu.CompilerParams(
             collective_id=0, has_side_effects=True, vmem_limit_bytes=67_000_000

time: 178 us -> 163 us (0.916)
  Pallas kernels: 173 us -> 158 us
    pallas_call x1, Pallas kernels: 173 us -> 158 us  [body(): pl.pallas_call(kernel, out_shape=jax.ShapeDtypeStruct((6, 256, 512), BF),...]
where the time goes in v2:
time: 163 us
  Pallas kernels  158 us (97%)
  other arithmetic  4.81 us (3%)
    pallas_call x1, Pallas kernels, body(): pl.pallas_call(kernel, out_shape=jax.ShapeDtypeStruct((6, 256, 512), BF),...  158 us
    convert_element_type x1, other arithmetic, body(): return result.astype(F32)  3.51 us

profile of v2, /device:TPU:1, one launch (start us, length us, event | category | flops | bytes accessed | tf_op | source)
XLA Modules:
  0.0 162.5 jit_solution(10170729361173440374)
XLA Ops:
  0.0 1.3 pad_convert_fusion.taps
  1.3 157.7 %mixers.1 = bf16[6,256,512]{2,1,0:T(8,128)(2,1)} custom-call(bf16[6,256,512]{2,1,0:T(8,128)(2,1)} %tokens.1, f32[3,2048]{1,0:T(4,128)} %gains.1, bf16[3,64,256]{2,1,0:T(8,128)(2,1)} %w_o.1, bf16[3,64,256]{2,1,0:T(8,128)(2,1)} %w_i.1, bf16[3,64,256]{2,1,0:T(8,128)(2,1)} %w_v.1, f32[3,8,256]{2,1,0:T(8,128)} %pad_convert_fusion.taps, bf16[3,32,512]{2,1,0:T(8,128)(2,1)} %w_u.1), custom_call_target="tpu_custom_call" | custom-call | tf_op jit(solution)/shard_map/mixers/pallas_call | solution.py:382
  159.0 3.5 %convert_element_type.6 = f32[6,256,512]{2,1,0:T(8,128)} convert(bf16[6,256,512]{2,1,0:T(8,128)(2,1)} %mixers.1) | non-fusion elementwise | flops 786432 | bytes 4718592 | tf_op jit(solution)/shard_map/convert_element_type | solution.py:404

commit v3 on v2

--- a/solution.py
+++ b/solution.py
@@ -18,14 +18,15 @@
 BF, F32 = jnp.bfloat16, jnp.float32
 
 ORDERS = (
-    ("xyz", "xyz", "xyz"),
-    ("yzx", "yzx", "yzx"),
-    ("zxy", "zxy", "zxy"),
-    ("xyz", "xyz", "xyz"),
-    ("xzy", "xzy", "xzy"),
+    "xyz",
+    "yzx",
+    "zxy",
+    "xyz",
+    "xzy",
 )
 NMAT = 5
 EVERY, PROJ, OUTP = (0, 1, 2, 3, 4), (0, 1, 2), (3, 4)
+ON_X, ON_YZ = (1,), (0, 2, 3, 4)
 
 
 class Sems:
@@ -36,7 +37,7 @@
         return self.at.setdefault(key, len(self.at))
 
 
-N_SEMS = 288
+N_SEMS = 296
 
 
 def kernel(
@@ -69,11 +70,11 @@
     def arrived(dst, key):
         remote(dst, dst, key, device(dc=1)).wait_recv()
 
-    def region(m, layer, full, moved=None, by=0, half=None, core=None):
+    def region(m, layer, full, moved=None, half=None, core=None):
         place = {"x": x, "y": y, "z": z}
         core = c if core is None else core
-        if moved is not None:
-            place[moved] = lax.rem(place[moved] + by + 4, 4)
+        for dim, step in (moved or {}).items():
+            place[dim] = lax.rem(place[dim] + step + 4, 4)
         pick = [slice(None) if d in full else place[d] for d in "xzy"]
         if m < 3:
             tail = slice(None) if half is None else pl.ds(half * 32, 32)
@@ -102,9 +103,11 @@
     pl.semaphore_wait(barrier, len(peers))
 
     for m in range(NMAT):
-        d = ORDERS[m][0][0]
         for s in (1, -1):
-            start(args[m], region(m, ALL, ""), (m, 1, s), neighbour(d, s))
+            start(args[m], region(m, ALL, ""), (m, 1, s), neighbour(ORDERS[m][0], s))
+    for m in range(NMAT):
+        for s in (1, -1):
+            start(args[m], region(m, ALL, ""), (m, 3, s, 0), neighbour(ORDERS[m][1], s))
 
     def rows_of(xd):
         return 3 * (xd // 2) + 2 * lax.rem(xd, 2), 3 * (xd // 2) + 1, lax.rem(xd, 2)
@@ -139,7 +142,7 @@
         else:
             pl.when(when)(action)
 
-    pltpu.make_async_copy(taps, t_buf.at[x], local.at[8]).start()
+    t_buf[x] = taps[...]
     for d in (1, 2, 3):
         start(taps, t_buf.at[x], ("taps", d), device(dx=d))
     token_list = token_copies()
@@ -175,55 +178,58 @@
         def _():
             x_buf[:, pl.ds(B0 - 16, 16), :] = jnp.zeros((4, 16, 512), BF)
 
-        pltpu.make_async_copy(taps, t_buf.at[x], local.at[8]).wait()
         for d in (1, 2, 3):
             arrived(t_buf.at[lax.rem(x - d + 4, 4)], ("taps", d))
 
-    for m in range(NMAT):
-        d = ORDERS[m][0][0]
+    def spread(m, by):
         for s in (1, -1):
-            arrived(region(m, ALL, "", d, -s), (m, 1, s))
-            part = region(m, ALL, "", d, -s, half=0 if s == 1 else 1)
+            block = region(m, ALL, "", {ORDERS[m][0]: by})
+            start(block, block, (m, 3, s, by), neighbour(ORDERS[m][1], s))
+
+    for m in range(NMAT):
+        d = ORDERS[m][0]
+        for s in (1, -1):
+            arrived(region(m, ALL, "", {d: -s}), (m, 1, s))
+            part = region(m, ALL, "", {d: -s}, half=0 if s == 1 else 1)
             start(part, part, (m, 2, s), neighbour(d, s))
     for m in range(NMAT):
+        spread(m, -1)
+        spread(m, 1)
+    for m in range(NMAT):
         own[m].wait()
+        for s in (1, -1):
+            arrived(region(m, ALL, "", {ORDERS[m][0]: 2}, half=0 if s == 1 else 1), (m, 2, s))
+        spread(m, 2)
 
     for layer in range(L):
         for m in range(NMAT):
-            first, d, _ = ORDERS[m][layer]
-            if layer == 0:
-                for s in (1, -1):
-                    arrived(region(m, ALL, "", first, -2 * s, half=0 if s == 1 else 1), (m, 2, s))
-            for s in (1, -1):
-                block = region(m, layer, first)
-                start(block, block, (m, layer, 3, s), neighbour(d, s))
-    for layer in range(L):
-        for m in range(NMAT):
-            first, d, _ = ORDERS[m][layer]
-            for s in (1, -1):
-                arrived(region(m, layer, first, d, -s), (m, layer, 3, s))
-                part = region(m, layer, first, d, -s, half=0 if s == 1 else 1)
+            first, d, _ = ORDERS[m]
+            for s in (1, -1):
+                if layer == 0:
+                    for by in (0, -1, 1, 2):
+                        arrived(region(m, ALL, "", {first: by, d: -s}), (m, 3, s, by))
+                part = region(m, layer, first, {d: -s}, half=0 if s == 1 else 1)
                 start(part, part, (m, layer, 4, s), neighbour(d, s))
 
     partner = device(dc=1)
 
     def second_done(layer):
         for m in range(NMAT):
-            first, d, _ = ORDERS[m][layer]
-            for s in (1, -1):
-                arrived(region(m, layer, first, d, -2 * s, half=0 if s == 1 else 1), (m, layer, 4, s))
+            first, d, _ = ORDERS[m]
+            for s in (1, -1):
+                arrived(region(m, layer, first, {d: 2}, half=0 if s == 1 else 1), (m, layer, 4, s))
 
     def third(layer, part, mats=EVERY):
         for m in mats:
-            first, second, d = ORDERS[m][layer]
+            first, second, d = ORDERS[m]
             for s in (1, -1):
                 half = part if s == 1 else 1 - part
                 block = region(m, layer, first + second, half=half)
                 start(block, block, (m, layer, 5 + part, s), neighbour(d, s))
 
     def across(m, layer, which, half=None):
-        first, second, d = ORDERS[m][layer]
-        block = region(m, layer, first + second, d, which, half)
+        first, second, d = ORDERS[m]
+        block = region(m, layer, first + second, {d: which}, half)
         start(block, block, (m, layer, "core", which, half), partner)
 
     def own_across(layer):
@@ -232,32 +238,32 @@
 
     def pass_on(layer, mats=EVERY):
         for m in mats:
-            first, second, d = ORDERS[m][layer]
-            for s in (1, -1):
-                part = region(m, layer, first + second, d, -s, half=0 if s == 1 else 1)
+            first, second, d = ORDERS[m]
+            for s in (1, -1):
+                part = region(m, layer, first + second, {d: -s}, half=0 if s == 1 else 1)
                 arrived(part, (m, layer, 5, s))
                 start(part, part, (m, layer, 7, s), neighbour(d, s))
 
     def near_done(layer, mats=EVERY):
         for m in mats:
-            first, second, d = ORDERS[m][layer]
-            for s in (1, -1):
-                arrived(region(m, layer, first + second, d, -s, half=1 if s == 1 else 0), (m, layer, 6, s))
+            first, second, d = ORDERS[m]
+            for s in (1, -1):
+                arrived(region(m, layer, first + second, {d: -s}, half=1 if s == 1 else 0), (m, layer, 6, s))
                 across(m, layer, -s)
 
     def far_done(layer, mats=EVERY):
         for m in mats:
-            first, second, d = ORDERS[m][layer]
+            first, second, d = ORDERS[m]
             for s in (1, -1):
                 half = 0 if s == 1 else 1
-                arrived(region(m, layer, first + second, d, 2, half=half), (m, layer, 7, s))
+                arrived(region(m, layer, first + second, {d: 2}, half=half), (m, layer, 7, s))
                 across(m, layer, 2, half)
 
     def from_partner(layer, mats=EVERY):
         for which, half in ((0, None), (1, None), (-1, None), (2, 0), (2, 1)):
             for m in mats:
-                first, second, d = ORDERS[m][layer]
-                block = region(m, layer, first + second, d, which, half, core=1 - c)
+                first, second, d = ORDERS[m]
+                block = region(m, layer, first + second, {d: which}, half, core=1 - c)
                 arrived(block, (m, layer, "core", which, half))
 
     def normalize(layer):
@@ -284,9 +290,10 @@
 
             g_buf[pl.ds(8, ROWS), :] = project(1) * project(2)
             outer = project(0)
+            tap = t_buf[b, layer].astype(F32)
             conved = jnp.zeros((ROWS, 256), F32)
             for k in range(3):
-                conved += t_buf[b, layer, pl.ds(k, 1), :] * g_buf[pl.ds(6 + k, ROWS), :]
+                conved += tap[k : k + 1, :] * g_buf[pl.ds(6 + k, ROWS), :]
             m_buf[:, pl.ds(pl.multiple_of(b * 256, 256), 256)] = (outer * conved).astype(BF)
             return 0
 
@@ -303,40 +310,52 @@
 
         lax.fori_loop(0, 4, step, 0)
 
+    start_tokens()
     second_done(0)
     third(0, 0)
     third(0, 1)
     own_across(0)
     second_done(1)
-    third(1, 0)
     own_across(1)
-    start_tokens()
     second_done(2)
     own_across(2)
-    pass_on(0)
-    third(1, 1)
-    third(2, 0, PROJ)
-    near_done(0)
-    far_done(0)
+    pass_on(0, ON_YZ)
+    third(1, 0, ON_YZ)
+    third(1, 1, ON_YZ)
     wait_tokens()
     normalize(0)
+    near_done(0, ON_YZ)
+    pass_on(0, ON_X)
+    third(1, 0, ON_X)
+    third(1, 1, ON_X)
+    near_done(0, ON_X)
+    far_done(0, ON_YZ)
+    far_done(0, ON_X)
     from_partner(0)
-    mix(0)
+    mix(0, 0, 2)
+    pass_on(1, ON_X)
+    third(2, 0, ON_X)
+    third(2, 1, ON_X)
+    pass_on(1, ON_YZ)
+    third(2, 0, (0, 2))
+    third(2, 1, (0, 2))
+    third(2, 0, OUTP)
+    mix(0, 2, 4)
+    near_done(1, ON_X)
     project_all(0)
-    pass_on(1)
-    third(2, 1, PROJ)
-    third(2, 0, OUTP)
+    near_done(1, ON_YZ)
     normalize(1)
-    near_done(1)
-    far_done(1)
+    far_done(1, ON_X)
+    far_done(1, ON_YZ)
     from_partner(1)
-    mix(1)
-    project_all(1)
+    mix(1, 0, 2)
     pass_on(2, PROJ)
     third(2, 1, OUTP)
+    mix(1, 2, 4)
+    near_done(2, PROJ)
+    project_all(1)
+    pass_on(2, OUTP)
     normalize(2)
-    pass_on(2, OUTP)
-    near_done(2, PROJ)
     far_done(2, PROJ)
     from_partner(2, PROJ)
     mix(2, 0, 2)
@@ -376,13 +395,12 @@
 
 
 def body(tokens, norm_gains, weight_outer, weight_inner, weight_value, conv_taps, weight_output):
-    taps = jnp.pad(conv_taps.astype(F32), ((0, 0), (0, 5), (0, 0)))
     hbm = pl.BlockSpec(memory_space=pl.ANY)
     vmem = pl.BlockSpec(memory_space=pltpu.VMEM)
     result = pl.pallas_call(
         kernel,
         out_shape=jax.ShapeDtypeStruct((6, 256, 512), BF),
-        in_specs=[hbm, vmem, hbm, hbm, hbm, hbm, hbm],
+        in_specs=[hbm, vmem, hbm, hbm, hbm, vmem, hbm],
         out_specs=hbm,
         scratch_shapes=[
             pltpu.VMEM((L, 3, 4, 4, 4, 2, 64, 256), BF),
@@ -391,16 +409,16 @@
             pltpu.VMEM((ROWS, 2048), BF),
             pltpu.VMEM((ROWS, 1024), BF),
             pltpu.VMEM((ROWS + 8, 256), F32),
-            pltpu.VMEM((4, 3, 8, 256), F32),
+            pltpu.VMEM((4, 3, 3, 256), BF),
             pltpu.SemaphoreType.DMA((N_SEMS,)),
             pltpu.SemaphoreType.DMA((N_SEMS,)),
-            pltpu.SemaphoreType.DMA((9,)),
+            pltpu.SemaphoreType.DMA((8,)),
         ],
         compiler_params=pltpu.CompilerParams(
             collective_id=0, has_side_effects=True, vmem_limit_bytes=67_000_000
         ),
         name="mixers",
-    )(tokens, norm_gains, weight_outer, weight_inner, weight_value, taps, weight_output)
+    )(tokens, norm_gains, weight_outer, weight_inner, weight_value, conv_taps, weight_output)
     return result.astype(F32)
 
 

time: 163 us -> 146 us (0.90)
  Pallas kernels: 158 us -> 142 us
    pallas_call x1, Pallas kernels: 158 us -> 142 us  [body(): pl.pallas_call(kernel, out_shape=jax.ShapeDtypeStruct((6, 256, 512), BF),...]
where the time goes in v3:
time: 146 us
  Pallas kernels  142 us (97%)
  other arithmetic  3.51 us (2%)
    pallas_call x1, Pallas kernels, body(): pl.pallas_call(kernel, out_shape=jax.ShapeDtypeStruct((6, 256, 512), BF),...  142 us
    convert_element_type x1, other arithmetic, body(): return result.astype(F32)  3.51 us

profile of v3, /device:TPU:1, one launch (start us, length us, event | category | flops | bytes accessed | tf_op | source)
XLA Modules:
  0.0 145.8 jit_solution(17764197203605383366)
XLA Ops:
  0.0 142.3 %mixers.1 = bf16[6,256,512]{2,1,0:T(8,128)(2,1)} custom-call(bf16[6,256,512]{2,1,0:T(8,128)(2,1)} %tokens.1, f32[3,2048]{1,0:T(4,128)} %gains.1, bf16[3,64,256]{2,1,0:T(8,128)(2,1)} %w_o.1, bf16[3,64,256]{2,1,0:T(8,128)(2,1)} %w_i.1, bf16[3,64,256]{2,1,0:T(8,128)(2,1)} %w_v.1, bf16[3,3,256]{2,1,0:T(4,128)(2,1)} %taps.1, bf16[3,32,512]{2,1,0:T(8,128)(2,1)} %w_u.1), custom_call_target="tpu_custom_call" | custom-call | tf_op jit(solution)/shard_map/mixers/pallas_call | solution.py:400
  142.3 3.5 %convert_element_type.3 = f32[6,256,512]{2,1,0:T(8,128)} convert(bf16[6,256,512]{2,1,0:T(8,128)(2,1)} %mixers.1) | non-fusion elementwise | flops 786432 | bytes 4718592 | tf_op jit(solution)/shard_map/convert_element_type | solution.py:422
